TPU v7x, 32 devices: a whole 2x2x4 slice. The times are simulated.
32 devices in a mesh: grp: 2 (over y), sp: 4 (over z), tp: 4 (over x, core).
Axes of the slice: x: 2, y: 2, z: 4, core: 2. Of those that a mesh axis runs over, the one named last changes fastest.
Arguments:
- starting_stream: bfloat16 [3072, 2048], P(('grp', 'sp'), 'tp'), parts along dimension 0, may hold values from -45 to 45
- multiplier_matrix: bfloat16 [2, 2048, 2048], P(None, 'sp', 'tp'), may hold values from -0.125 to 0.125
- memory_path_matrix: bfloat16 [2, 2048, 2048], P(None, 'sp', 'tp'), may hold values from -0.125 to 0.125
- filter_coefficients: bfloat16 [2, 4, 2048], P(None, None, 'tp'), may hold values from -3 to 3
- memory_valve_matrix: bfloat16 [2, 8, 256, 256], P(None, 'tp'), may hold values from -0.375 to 0.375
- entry_valve_matrix: bfloat16 [2, 8, 256, 256], P(None, 'tp'), may hold values from -0.375 to 0.375
- forgetting_parameters: float32 [2, 2048], P(None, 'tp'), may hold values from 3 to 15
- timestep_forgetting_multiplier: float32 [3072], P(('grp', 'sp')), parts along dimension 0, may hold values from 0.5 to 2
- spike_extra: float32 [3072, 2048], P(('grp', 'sp'), 'tp'), parts along dimension 0, may hold values from -0.7 to 0
- exit_projector_matrix: bfloat16 [2, 2048, 2048], P(None, 'tp', 'sp'), may hold values from -0.125 to 0.125
- prelude_rms_gains: float32 [2, 2048], replicated, may hold values from 0.1 to 1.9
- finishing_rms_gains: float32 [2048], P('tp'), may hold values from 0.1 to 1.9
Outputs:
- result: bfloat16 [3072, 2048], P(('grp', 'sp'), 'tp'), parts along dimension 0
There are 2 independent parts, one for each index of `grp`. A program takes and returns all parts, laid end to end along the dimension named above; an argument that names none is the same for every part. Nothing has to cross between parts.
All inputs are finite; a program needn't handle non-finite values.
Results may differ from a plain program's by a relative error of at most 0.015.
Values may be sent and summed in bfloat16 or wider, within the bound.
A program may use at most 64 MiB of HBM per device.

v0:
```python
import jax
import jax.numpy as jnp
from jax import lax
from jax.sharding import PartitionSpec as P

BLOCK_W = 256


EPSILON = 1e-06
SQUASH_POWER = 8.0


def from_behind(value, axis, steps):
    count = lax.axis_size(axis)
    first, last = (max(0, -steps), min(count, count - steps))
    return lax.ppermute(value, axis, [(source, source + steps) for source in range(first, last)])


def entering(part, axis, combine, identity):
    place = lax.axis_index(axis)
    gathered = jax.tree.map(lambda a: lax.all_gather(a, axis), part)
    state = jax.tree.map(lambda a, e: jnp.zeros_like(a) + jnp.asarray(e, a.dtype), part, identity)

    def one(lap, state):
        return combine(
            state, jax.tree.map(lambda a: lax.dynamic_index_in_dim(a, lap, 0, False), gathered)
        )

    return lax.fori_loop(0, place, one, state)


def combine_pairs(earlier, later):
    return (earlier[0] * later[0], later[0] * earlier[1] + later[1])


def gather_rows(own_cols):
    return lax.all_gather(own_cols, "tp", axis=1, tiled=True)


def on_device(
    starting_stream,
    multiplier_matrix,
    memory_path_matrix,
    filter_coefficients,
    memory_valve_matrix,
    entry_valve_matrix,
    forgetting_parameters,
    timestep_forgetting_multiplier,
    spike_extra,
    exit_projector_matrix,
    prelude_rms_gains,
    finishing_rms_gains,
):
    tok_rows = starting_stream.shape[0]
    channels = memory_path_matrix.shape[2]
    own_cols = starting_stream
    full_rows = gather_rows(starting_stream)
    for tier_number in range(memory_path_matrix.shape[0]):
        floats = full_rows.astype(jnp.float32)
        mean_square = jnp.mean(floats * floats, axis=1, keepdims=True)
        normed = (
            floats * lax.rsqrt(mean_square + EPSILON) * prelude_rms_gains[tier_number][None, :]
        ).astype(jnp.bfloat16)
        branch_acc = jnp.dot(
            normed,
            lax.all_gather(multiplier_matrix[tier_number], "sp", axis=0, tiled=True),
            preferred_element_type=jnp.float32,
        )
        recur_acc = jnp.dot(
            normed,
            lax.all_gather(memory_path_matrix[tier_number], "sp", axis=0, tiled=True),
            preferred_element_type=jnp.float32,
        )
        branch = branch_acc.astype(jnp.bfloat16)
        recurrent = recur_acc.astype(jnp.bfloat16)
        taps_now = filter_coefficients[tier_number]
        reach_back = taps_now.shape[0] - 1
        halo_rows = from_behind(recurrent[tok_rows - reach_back :], "sp", 1)
        extended = jnp.concatenate([halo_rows, recurrent], axis=0)
        conv_sum = jnp.zeros((tok_rows, channels), jnp.float32)
        for offset in range(taps_now.shape[0]):
            conv_sum = conv_sum + extended[offset : offset + tok_rows].astype(
                jnp.float32
            ) * taps_now[offset].astype(jnp.float32)
        convolved = conv_sum.astype(jnp.bfloat16)
        blocks = convolved.reshape(tok_rows, channels // BLOCK_W, BLOCK_W)
        reset_gate = jax.nn.sigmoid(
            jnp.einsum(
                "tnc,ncd->tnd",
                blocks,
                memory_valve_matrix[tier_number],
                preferred_element_type=jnp.float32,
            ).reshape(tok_rows, channels)
        )
        inject = jax.nn.sigmoid(
            jnp.einsum(
                "tnc,ncd->tnd",
                blocks,
                entry_valve_matrix[tier_number],
                preferred_element_type=jnp.float32,
            ).reshape(tok_rows, channels)
        )
        logarithmic_persistence = (
            -SQUASH_POWER
            * reset_gate
            * jax.nn.softplus(-forgetting_parameters[tier_number])[None, :]
            * timestep_forgetting_multiplier[:, None]
            + spike_extra
        )
        keep_rate = jnp.exp(logarithmic_persistence)
        driven = (
            inject
            * convolved.astype(jnp.float32)
            * jnp.sqrt(-jnp.expm1(2.0 * logarithmic_persistence))
        )
        keep_cum, state_local = lax.associative_scan(combine_pairs, (keep_rate, driven), axis=0)
        identity = (jnp.ones((channels,), jnp.float32), jnp.zeros((channels,), jnp.float32))
        carried = entering((keep_cum[-1], state_local[-1]), "sp", combine_pairs, identity)
        state_seq = state_local + keep_cum * carried[1][None, :]
        mixed_in = (jax.nn.gelu(branch.astype(jnp.float32)) * state_seq).astype(jnp.bfloat16)
        partial_value = jnp.dot(
            mixed_in,
            lax.all_gather(exit_projector_matrix[tier_number], "sp", axis=1, tiled=True),
            preferred_element_type=jnp.float32,
        )
        mixed_sum = lax.psum_scatter(
            partial_value.astype(jnp.bfloat16), "tp", scatter_dimension=1, tiled=True
        ).astype(jnp.float32)
        own_cols = (own_cols.astype(jnp.float32) + mixed_sum).astype(jnp.bfloat16)
        if tier_number + 1 < memory_path_matrix.shape[0]:
            full_rows = gather_rows(own_cols)
    floats = own_cols.astype(jnp.float32)
    full_width = floats.shape[1] * lax.axis_size("tp")
    square_sum = lax.psum(jnp.sum(floats * floats, axis=1), "tp")
    inv_rms = lax.rsqrt(square_sum / full_width + EPSILON)
    return (floats * inv_rms[:, None] * finishing_rms_gains[None, :]).astype(jnp.bfloat16)


def solution(mesh):
    return jax.shard_map(
        on_device,
        mesh=mesh,
        in_specs=(
            P(("grp", "sp"), "tp"),
            P(None, "sp", "tp"),
            P(None, "sp", "tp"),
            P(None, None, "tp"),
            P(None, "tp", None, None),
            P(None, "tp", None, None),
            P(None, "tp"),
            P(("grp", "sp")),
            P(("grp", "sp"), "tp"),
            P(None, "tp", "sp"),
            P(),
            P("tp"),
        ),
        out_specs=P(("grp", "sp"), "tp"),
        check_vma=False,
    )
```

profile of v0, /device:TPU:0, one launch (start us, length us, event | category | flops | bytes accessed | tf_op | source)
XLA Modules:
  0.0 496.0 jit_solution(4783613466114738588)
XLA Ops:
  7.3 2.3 fusion.151
  13.5 17.8 %all-gather.19.cloned.1.call-done = bf16[384,2048]{1,0:T(8,128)(2,1)} async-done(((bf16[384,512]{1,0:T(8,128)(2,1)}), bf16[384,2048]{1,0:T(8,128)(2,1)}) %all-gather.19.cloned.1.call-update) | async-done | bytes 1572880 | tf_op jit(solution)/shard_map/all_gather | solution.py:37
  33.1 45.5 %all-gather.25.cloned.1.call-done = bf16[1,2048,512]{2,1,0:T(8,128)(2,1)} async-done(((bf16[1,512,512]{2,1,0:T(8,128)(2,1)}), bf16[1,2048,512]{2,1,0:T(8,128)(2,1)}) %all-gather.25.cloned.1.call-update) | async-done | bytes 2097168 | tf_op jit(solution)/shard_map/all_gather | solution.py:71
  78.5 3.1 fusion.31
  81.7 2.1 collective-permute-start
  170.5 1.9 pad.217
  174.3 1.9 pad.201
  181.7 2.0 pad.218
  183.7 2.0 pad.219
  185.7 2.0 pad.203
  189.1 2.0 pad.202
  196.8 2.1 pad.220
  198.9 2.1 pad.221
  202.5 2.1 pad.204
  204.5 2.1 pad.205
  222.2 1.9 pad.210
  224.8 12.9 %all-gather.7 = f32[4,1,512]{2,1,0:T(1,128)S(1)} all-gather(f32[1,1,512]{2,1,0:T(1,128)S(1)} %add_bitcast_fusion.2), channel_id=1, replica_groups=mesh['grp'=2,'sp'=4,'tp'=4] {'sp'}, dimensions={0}, use_global_device_ids=true | all-gather | bytes 10240 | tf_op jit(solution)/shard_map/all_gather | solution.py:21
  237.7 1.9 pad.227
  240.6 11.9 %all-gather.6 = f32[4,1,512]{2,1,0:T(1,128)S(1)} all-gather(f32[1,1,512]{2,1,0:T(1,128)S(1)} %add_bitcast_fusion.3), channel_id=1, replica_groups=mesh['grp'=2,'sp'=4,'tp'=4] {'sp'}, dimensions={0}, use_global_device_ids=true | all-gather | bytes 10240 | tf_op jit(solution)/shard_map/all_gather | solution.py:21
  252.6 6.3 %convolution_convert_fusion.1 = bf16[384,2048]{1,0:T(8,128)(2,1)} fusion(bf16[1,512,2048]{2,1,0:T(8,128)(2,1)} %all-gather.27.cloned.1.call-done, bf16[1,2048,512]{2,1,0:T(8,128)(2,1)} %all-gather.23.cloned.1.call-done, f32[384,512]{1,0:T(8,128)S(1)} %pad.226, f32[384,512]{1,0:T(8,128)} %pad.227, f32[384,512]{1,0:T(8,128)} %pad.210, f32[384,512]{1,0:T(8,128)} %pad.211, ...), kind=kOutput, calls=%fused_computation.17 | convolution fusion | flops 1617690624 | bytes 10497536 | tf_op jit(solution)/shard_map/dot_general | solution.py:121
  259.0 26.7 %reduce-scatter.3.cloned.1.call-done = bf16[384,512]{1,0:T(8,128)(2,1)} async-done(((bf16[384,2048]{1,0:T(8,128)(2,1)}), bf16[384,512]{1,0:T(8,128)(2,1)}) %reduce-scatter.3.cloned.1.call-update) | async-done | bytes 393232 | tf_op jit(solution)/shard_map/reduce_scatter | solution.py:126
  289.3 18.1 %all-gather.21.cloned.1.call-done = bf16[384,2048]{1,0:T(8,128)(2,1)} async-done(((bf16[384,512]{1,0:T(8,128)(2,1)}), bf16[384,2048]{1,0:T(8,128)(2,1)}) %all-gather.21.cloned.1.call-update) | async-done | bytes 1572880 | tf_op jit(solution)/shard_map/all_gather | solution.py:37
  309.2 45.5 %all-gather.31.cloned.1.call-done = bf16[1,2048,512]{2,1,0:T(8,128)(2,1)} async-done(((bf16[1,512,512]{2,1,0:T(8,128)(2,1)}), bf16[1,2048,512]{2,1,0:T(8,128)(2,1)}) %all-gather.31.cloned.1.call-update) | async-done | bytes 2097168 | tf_op jit(solution)/shard_map/all_gather | solution.py:71
  354.6 3.2 fusion.37
  357.8 2.1 collective-permute-start.1
  385.4 13.6 %all-gather.9 = f32[4,1,512]{2,1,0:T(1,128)S(1)} all-gather(f32[1,1,512]{2,1,0:T(1,128)S(1)} %add_bitcast_fusion), channel_id=1, replica_groups=mesh['grp'=2,'sp'=4,'tp'=4] {'sp'}, dimensions={0}, use_global_device_ids=true | all-gather | bytes 10240 | tf_op jit(solution)/shard_map/all_gather | solution.py:21
  400.9 2.0 pad.258
  403.6 12.2 %all-gather.8 = f32[4,1,512]{2,1,0:T(1,128)S(1)} all-gather(f32[1,1,512]{2,1,0:T(1,128)S(1)} %add_bitcast_fusion.1), channel_id=1, replica_groups=mesh['grp'=2,'sp'=4,'tp'=4] {'sp'}, dimensions={0}, use_global_device_ids=true | all-gather | bytes 10240 | tf_op jit(solution)/shard_map/all_gather | solution.py:21
  415.8 31.0 %all-gather.33.cloned.1.call-done = bf16[1,512,2048]{2,1,0:T(8,128)(2,1)} async-done(((bf16[1,512,512]{2,1,0:T(8,128)(2,1)}), bf16[1,512,2048]{2,1,0:T(8,128)(2,1)}) %all-gather.33.cloned.1.call-update) | async-done | bytes 2097168 | tf_op jit(solution)/shard_map/all_gather | solution.py:123
  446.9 6.4 %convolution_convert_fusion = bf16[384,2048]{1,0:T(8,128)(2,1)} fusion(bf16[1,512,2048]{2,1,0:T(8,128)(2,1)} %all-gather.33.cloned.1.call-done, bf16[1,2048,512]{2,1,0:T(8,128)(2,1)} %all-gather.29.cloned.1.call-done, f32[384,512]{1,0:T(8,128)} %pad.258, f32[384,512]{1,0:T(8,128)} %pad.259, f32[384,512]{1,0:T(8,128)} %pad.242, ...), kind=kOutput, calls=%fused_computation.16 | convolution fusion | flops 1617690624 | bytes 10497536 | tf_op jit(solution)/shard_map/dot_general | solution.py:121
  453.3 27.0 %reduce-scatter.5.cloned.1.call-done = bf16[384,512]{1,0:T(8,128)(2,1)} async-done(((bf16[384,2048]{1,0:T(8,128)(2,1)}), bf16[384,512]{1,0:T(8,128)(2,1)}) %reduce-scatter.5.cloned.1.call-update) | async-done | bytes 393232 | tf_op jit(solution)/shard_map/reduce_scatter | solution.py:126
  481.5 5.8 %psum.7 = f32[384]{0:T(512)S(1)} all-reduce(f32[384]{0:T(512)S(1)} %fusion.40), channel_id=1, replica_groups=mesh['grp'=2,'sp'=4,'tp'=4] {'tp'}, use_global_device_ids=true, to_apply=%region_9.10 | all-reduce | flops 384 | bytes 3072 | tf_op jit(solution)/shard_map/psum | solution.py:134
  (381 shorter events, 161.8 us)
Async XLA Ops:
  6.5 24.7 %all-gather.19.cloned.1.call-start = ((), (), s32[]{:S(2)}) async-start(), calls=%async_computation.2 | async-start | bytes 1966080 | tf_op jit(solution)/shard_map/all_gather | solution.py:37
  7.3 71.3 %all-gather.25.cloned.1.call-start = ((), (), s32[]{:S(2)}) async-start(), calls=%async_computation.7 | async-start | bytes 2621440 | tf_op jit(solution)/shard_map/all_gather | solution.py:71
  9.6 242.9 %all-gather.23.cloned.1.call-start = ((), (), s32[]{:S(2)}) async-start(), calls=%async_computation.6 | async-start | bytes 2621440 | tf_op jit(solution)/shard_map/all_gather | solution.py:66
  10.8 241.8 %all-gather.27.cloned.1.call-start = ((), (), s32[]{:S(2)}) async-start(), calls=%async_computation.8 | async-start | bytes 2621440 | tf_op jit(solution)/shard_map/all_gather | solution.py:123
  12.2 273.5 %reduce-scatter.3.cloned.1.call-start = ((), (), s32[]{:S(2)}) async-start(), calls=%async_computation.3 | async-start | bytes 1966080 | tf_op jit(solution)/shard_map/reduce_scatter | solution.py:126
  12.9 68.8 %copy-start.24 = (f32[1,2048]{1,0:T(1,128)}, f32[1,2048]{1,0:T(1,128)S(1)}, u32[]{:S(2)}) copy-start(f32[1,2048]{1,0:T(1,128)S(1)} %get-tuple-element.182) | copy-start | bytes 24580
  33.1 45.5 %copy-start.29 = (f32[384]{0:T(512)}, f32[384]{0:T(512)S(1)}, u32[]{:S(2)}) copy-start(f32[384]{0:T(512)S(1)} %add_rsqrt_fusion.2) | copy-start | bytes 4612
  78.5 5.3 %copy-start.25 = (f32[2,512]{1,0:T(2,128)S(1)}, f32[2,512]{1,0:T(2,128)}, u32[]{:S(2)}) copy-start(f32[2,512]{1,0:T(2,128)} %param.22) | copy-start | bytes 12292
  78.5 7.0 %copy-start.31 = (bf16[2,2,256,256]{3,2,1,0:T(8,128)(2,1)S(1)}, bf16[2,2,256,256]{3,2,1,0:T(8,128)(2,1)}, u32[]{:S(2)}) copy-start(bf16[2,2,256,256]{3,2,1,0:T(8,128)(2,1)} %param.21) | copy-start | bytes 1572868
  81.7 3.4 collective-permute-start
  222.1 15.7 %copy-start.5 = (f32[192,512]{1,0:T(8,128)S(1)}, f32[192,512]{1,0:T(8,128)}, u32[]{:S(2)}) copy-start(f32[192,512]{1,0:T(8,128)} %add.500) | copy-start | bytes 1179652
  222.1 30.4 %copy-start.2 = (bf16[384,2048]{1,0:T(8,128)(2,1)S(1)}, bf16[384,2048]{1,0:T(8,128)(2,1)}, u32[]{:S(2)}) copy-start(bf16[384,2048]{1,0:T(8,128)(2,1)} %all-gather.19.cloned.1.call-done) | copy-start | bytes 4718596
  222.2 30.4 %copy-start.30 = (f32[384]{0:T(512)S(1)}, f32[384]{0:T(512)}, u32[]{:S(2)}) copy-start(f32[384]{0:T(512)} %copy-done.29) | copy-start | bytes 4612
  252.6 33.1 %copy-start.4 = (bf16[384,512]{1,0:T(8,128)(2,1)S(1)}, bf16[384,512]{1,0:T(8,128)(2,1)}, u32[]{:S(2)}) copy-start(bf16[384,512]{1,0:T(8,128)(2,1)} %param.16) | copy-start | bytes 1179652
  258.9 95.7 %copy-start.23 = (f32[1,2048]{1,0:T(1,128)S(1)}, f32[1,2048]{1,0:T(1,128)}, u32[]{:S(2)}) copy-start(f32[1,2048]{1,0:T(1,128)} %get-tuple-element.181) | copy-start | bytes 24580
  258.9 48.4 %all-gather.21.cloned.1.call-start = ((), (), s32[]{:S(2)}) async-start(), calls=%async_computation.4 | async-start | bytes 1966080 | tf_op jit(solution)/shard_map/all_gather | solution.py:37
  287.6 67.0 %all-gather.31.cloned.1.call-start = ((), (), s32[]{:S(2)}) async-start(), calls=%async_computation.10 | async-start | bytes 2621440 | tf_op jit(solution)/shard_map/all_gather | solution.py:71
  288.3 127.5 %all-gather.29.cloned.1.call-start = ((), (), s32[]{:S(2)}) async-start(), calls=%async_computation.9 | async-start | bytes 2621440 | tf_op jit(solution)/shard_map/all_gather | solution.py:66
  289.1 157.8 %all-gather.33.cloned.1.call-start = ((), (), s32[]{:S(2)}) async-start(), calls=%async_computation.11 | async-start | bytes 2621440 | tf_op jit(solution)/shard_map/all_gather | solution.py:123
  309.1 48.6 %copy-start.27 = (f32[384]{0:T(512)}, f32[384]{0:T(512)S(1)}, u32[]{:S(2)}) copy-start(f32[384]{0:T(512)S(1)} %add_rsqrt_fusion.1) | copy-start | bytes 4612
  354.6 6.6 %copy-start.19 = (f32[1,1,512]{2,1,0:T(1,128)S(1)}, f32[1,1,512]{2,1,0:T(1,128)}, u32[]{:S(2)}) copy-start(f32[1,1,512]{2,1,0:T(1,128)} %get-tuple-element.193) | copy-start | bytes 6148
  354.6 6.6 %copy-start.20 = (f32[1,1,512]{2,1,0:T(1,128)S(1)}, f32[1,1,512]{2,1,0:T(1,128)}, u32[]{:S(2)}) copy-start(f32[1,1,512]{2,1,0:T(1,128)} %get-tuple-element.194) | copy-start | bytes 6148
  354.6 6.6 %copy-start.21 = (f32[1,1,512]{2,1,0:T(1,128)S(1)}, f32[1,1,512]{2,1,0:T(1,128)}, u32[]{:S(2)}) copy-start(f32[1,1,512]{2,1,0:T(1,128)} %get-tuple-element.199) | copy-start | bytes 6148
  354.6 6.6 %copy-start.22 = (f32[1,1,512]{2,1,0:T(1,128)S(1)}, f32[1,1,512]{2,1,0:T(1,128)}, u32[]{:S(2)}) copy-start(f32[1,1,512]{2,1,0:T(1,128)} %get-tuple-element.200) | copy-start | bytes 6148
  354.6 7.0 %copy-start.32 = (bf16[2,2,256,256]{3,2,1,0:T(8,128)(2,1)S(1)}, bf16[2,2,256,256]{3,2,1,0:T(8,128)(2,1)}, u32[]{:S(2)}) copy-start(bf16[2,2,256,256]{3,2,1,0:T(8,128)(2,1)} %param.21) | copy-start | bytes 1572868
  357.8 3.4 collective-permute-start.1
  359.9 120.4 %reduce-scatter.5.cloned.1.call-start = ((), (), s32[]{:S(2)}) async-start(), calls=%async_computation.5 | async-start | bytes 1966080 | tf_op jit(solution)/shard_map/reduce_scatter | solution.py:126
  382.8 64.1 %copy-start.3 = (bf16[384,2048]{1,0:T(8,128)(2,1)S(1)}, bf16[384,2048]{1,0:T(8,128)(2,1)}, u32[]{:S(2)}) copy-start(bf16[384,2048]{1,0:T(8,128)(2,1)} %all-gather.21.cloned.1.call-done) | copy-start | bytes 4718596
  382.8 64.1 %copy-start.8 = (f32[384,512]{1,0:T(8,128)S(1)}, f32[384,512]{1,0:T(8,128)}, u32[]{:S(2)}) copy-start(f32[384,512]{1,0:T(8,128)} %pad.243) | copy-start | bytes 2359300
  382.8 64.1 %copy-start.28 = (f32[384]{0:T(512)S(1)}, f32[384]{0:T(512)}, u32[]{:S(2)}) copy-start(f32[384]{0:T(512)} %copy-done.27) | copy-start | bytes 4612
  446.9 33.4 %copy-start = (bf16[384,512]{1,0:T(8,128)(2,1)S(1)}, bf16[384,512]{1,0:T(8,128)(2,1)}, u32[]{:S(2)}) copy-start(bf16[384,512]{1,0:T(8,128)(2,1)} %add_convert_fusion.2) | copy-start | bytes 1179652
  453.3 34.0 %copy-start.26 = (f32[512]{0:T(512)S(1)}, f32[512]{0:T(512)}, u32[]{:S(2)}) copy-start(f32[512]{0:T(512)} %param.27) | copy-start | bytes 6148
  (15 other events, 28.0 us)
Sparse Core Ops, SparseCore 0:
  8.9 22.3 all-gather.18
  32.8 45.6 all-gather.24
  80.1 44.4 all-gather.22
  126.0 44.4 all-gather.26
  259.0 26.6 reduce-scatter.2
  287.7 19.6 all-gather.20
  308.9 45.6 all-gather.30
  356.2 44.5 all-gather.28
  402.4 44.4 all-gather.32
  453.5 26.8 reduce-scatter.4
where the time goes:
time: 501 us; the launch traced here: 496 us
  waiting for transfers between devices  216 us (43%)
  local copies, waits for them, and re-layouts  118 us (24%)
  other arithmetic  65.8 us (13%)
  blocking collectives  56.4 us (11%)
  matrix products  20.7 us (4%)
  between operations  14.9 us (3%)
    all_gather x2, waiting for transfers between devices, on_device(): lax.all_gather(memory_path_matrix[tier_number], 'sp', axis=0, tiled=True)  90.9 us
    slice x112, local copies, waits for them, and re-layouts, on_device(): lax.associative_scan(combine_pairs, (keep_rate, driven), axis=0)  61.7 us
    reduce_scatter x2, waiting for transfers between devices, on_device(): lax.psum_scatter(partial_value.astype(jnp.bfloat16), 'tp', scatter_dimens...  53.7 us
    all_gather x4, blocking collectives, entering(): gathered = jax.tree.map(lambda a: lax.all_gather(a, axis), part)  50.6 us
    pad x60, local copies, waits for them, and re-layouts, on_device(): lax.associative_scan(combine_pairs, (keep_rate, driven), axis=0)  46.7 us
    all_gather x2, waiting for transfers between devices, gather_rows(): return lax.all_gather(own_cols, 'tp', axis=1, tiled=True)  35.9 us
    all_gather x2, waiting for transfers between devices, on_device(): lax.all_gather(exit_projector_matrix[tier_number], 'sp', axis=1, tiled=True)  31.1 us
    add x30, other arithmetic, combine_pairs(): return (earlier[0] * later[0], later[0] * earlier[1] + later[1])  19.8 us
  transfers between devices with their start and end apart: 12, of which 9 were waited for; matrix products, arithmetic and copies ran while one was open for 37% of the time, Pallas kernels for 0%

commit v1 on v0

--- a/solution.py
+++ b/solution.py
@@ -1,6 +1,10 @@
+import functools
+
 import jax
 import jax.numpy as jnp
 from jax import lax
+from jax.experimental import pallas as pl
+from jax.experimental.pallas import tpu as pltpu
 from jax.sharding import PartitionSpec as P
 
 BLOCK_W = 256
@@ -136,9 +140,572 @@
     return (floats * inv_rms[:, None] * finishing_rms_gains[None, :]).astype(jnp.bfloat16)
 
 
+MESH = pl.DeviceIdType.MESH
+F32, BF16 = jnp.float32, jnp.bfloat16
+
+
+def one_minus_exp(u):
+    series = -u * (
+        1 + u / 2 * (1 + u / 3 * (1 + u / 4 * (1 + u / 5 * (1 + u / 6 * (1 + u / 7)))))
+    )
+    return jnp.where(u > -0.35, series, 1.0 - jnp.exp(u))
+
+
+def shifted(value, steps, fill):
+    rows = value.shape[0]
+    if steps % 8 == 0:
+        top = jnp.full((steps, value.shape[1]), fill, value.dtype)
+        return jnp.concatenate([top, value[: rows - steps]], axis=0)
+    at = lax.broadcasted_iota(jnp.int32, value.shape, 0)
+    return jnp.where(at < steps, fill, pltpu.roll(value, steps, 0))
+
+
+def fused(
+    sizes,
+    x_ref,
+    branch_w,
+    memory_w,
+    exit_w,
+    taps_ref,
+    reset_w,
+    inject_w,
+    rate_ref,
+    mult_ref,
+    spike_ref,
+    gains_ref,
+    final_ref,
+    out_ref,
+    win,
+    wout,
+    agx,
+    xs,
+    nrm,
+    ext,
+    halo,
+    keep_s,
+    state_s,
+    gel_s,
+    mix_s,
+    part,
+    from_sib,
+    pair,
+    from_far,
+    cry_out,
+    cry_in,
+    hacc,
+    sq_out,
+    sq_in,
+    sem_own,
+    sem_w_recv,
+    sem_up,
+    sem_down,
+    sem_y,
+    sem_ag_send,
+    sem_ag_recv,
+    sem_rs_send,
+    sem_rs_recv,
+    sem_h,
+    sem_c_send,
+    sem_c_recv,
+    sem_q_send,
+    sem_q_recv,
+):
+    layers, n_sp, n_tp, n_grp, rows, chans, feats, depth, pieces = sizes
+    chips = n_tp // 2
+    g, s, t = lax.axis_index("grp"), lax.axis_index("sp"), lax.axis_index("tp")
+    core = lax.rem(t, 2)
+    chip = t // 2
+    sib = chip * 2 + 1 - core
+    full = n_tp * feats
+
+    def up():
+        return {"sp": s + 1}
+
+    def down():
+        return {"sp": s - 1}
+
+    def across():
+        return {"grp": 1 - g}
+
+    barrier = pltpu.get_barrier_semaphore()
+    for d in range(1, n_tp):
+        pl.semaphore_signal(
+            barrier, inc=1, device_id={"tp": lax.rem(t + d, n_tp)}, device_id_type=MESH
+        )
+    for d in range(1, n_sp):
+        pl.semaphore_signal(
+            barrier, inc=1, device_id={"sp": lax.rem(s + d, n_sp)}, device_id_type=MESH
+        )
+    pl.semaphore_signal(barrier, inc=1, device_id=across(), device_id_type=MESH)
+    pl.semaphore_wait(barrier, n_tp - 1 + n_sp - 1 + 1)
+
+    def own_block(m):
+        return (memory_w, branch_w, exit_w)[m % 3].at[m // 3]
+
+    def held(m, j):
+        return win.at[2 * (m // 3) + m % 3, j] if m % 3 < 2 else wout.at[m // 3, j]
+
+    def sent(src, m, j, half, send_sem, where):
+        return pltpu.make_async_remote_copy(
+            src_ref=src,
+            dst_ref=held(m, j).at[half],
+            send_sem=send_sem.at[m, j],
+            recv_sem=sem_w_recv.at[m, j, half],
+            device_id=where,
+            device_id_type=MESH,
+        )
+
+    def start_own(m):
+        src = own_block(m).at[g]
+
+        @pl.when(s < n_sp - 1)
+        def _():
+            sent(src, m, s, g, sem_up, up()).start()
+
+        @pl.when(s > 0)
+        def _():
+            sent(src, m, s, g, sem_down, down()).start()
+
+    def keep_own(m):
+        return pltpu.make_async_copy(own_block(m), held(m, s), sem_own.at[m])
+
+    def pump(m):
+        for d in range(1, n_sp):
+
+            @pl.when(s - d >= 0)
+            def _():
+                j = s - d
+                src = held(m, j).at[g]
+                sent(src, m, j, g, sem_up, up()).wait_recv()
+
+                @pl.when(s < n_sp - 1)
+                def _():
+                    sent(src, m, j, g, sem_up, up()).start()
+
+                sent(src, m, j, g, sem_y, across()).start()
+
+            @pl.when(s + d < n_sp)
+            def _():
+                j = s + d
+                src = held(m, j).at[g]
+                sent(src, m, j, g, sem_down, down()).wait_recv()
+
+                @pl.when(s > 0)
+                def _():
+                    sent(src, m, j, g, sem_down, down()).start()
+
+                sent(src, m, j, g, sem_y, across()).start()
+
+        if m + 3 < 3 * layers:
+            start_own(m + 3)
+
+    def arrived(m):
+        keep_own(m).wait()
+        for d in range(1, n_sp):
+            j = lax.rem(s + d, n_sp)
+            src = held(m, j).at[1 - g]
+            sent(src, m, j, 1 - g, sem_y, across()).wait_recv()
+
+    def close_weights():
+        for m in range(3 * layers):
+            for j in range(n_sp):
+                src = held(m, j).at[g]
+
+                @pl.when((s < n_sp - 1) & (j <= s))
+                def _():
+                    sent(src, m, j, g, sem_up, up()).wait_send()
+
+                @pl.when((s > 0) & (j >= s))
+                def _():
+                    sent(src, m, j, g, sem_down, down()).wait_send()
+
+                @pl.when(j != s)
+                def _():
+                    sent(src, m, j, g, sem_y, across()).wait_send()
+
+    for m in range(3 * layers):
+        keep_own(m).start()
+
+    def ag_copy(src, layer, owner, k, where):
+        return pltpu.make_async_remote_copy(
+            src_ref=src,
+            dst_ref=agx.at[layer, owner],
+            send_sem=sem_ag_send.at[layer, k],
+            recv_sem=sem_ag_recv.at[layer, owner],
+            device_id={"tp": where},
+            device_id_type=MESH,
+        )
+
+    def ag_start(layer, src):
+        for d in range(1, chips):
+            ag_copy(src, layer, t, d, lax.rem(t + 2 * d, n_tp)).start()
+        ag_copy(src, layer, t, 0, sib).start()
+
+    def ag_finish(layer, src):
+        for d in range(1, chips):
+            owner = lax.rem(t + 2 * d, n_tp)
+            block = agx.at[layer, owner]
+            ag_copy(block, layer, owner, d, sib).wait_recv()
+            ag_copy(block, layer, owner, chips + d, sib).start()
+        ag_copy(src, layer, sib, 0, sib).wait_recv()
+        for d in range(1, chips):
+            owner = lax.rem(sib + 2 * d, n_tp)
+            ag_copy(agx.at[layer, owner], layer, owner, d, sib).wait_recv()
+
+    def ag_close(layer, src):
+        for d in range(1, chips):
+            ag_copy(src, layer, t, d, sib).wait_send()
+            ag_copy(src, layer, t, chips + d, sib).wait_send()
+        ag_copy(src, layer, t, 0, sib).wait_send()
+
+    ag_start(0, x_ref)
+    for m in range(min(3, 3 * layers)):
+        start_own(m)
+
+    step = rows // pieces
+
+    def normalize(layer):
+        def one(i, carry):
+            at = pl.ds(pl.multiple_of(i * step, step), step)
+            total = jnp.zeros((step, 1), F32)
+            for p in range(n_tp):
+                f = agx[layer, p, at].astype(F32)
+                total = total + jnp.sum(f * f, axis=1, keepdims=True)
+            inv = lax.rsqrt(total / full + EPSILON)
+            for p in range(n_tp):
+                cols = slice(p * feats, (p + 1) * feats)
+                f = agx[layer, p, at].astype(F32)
+                gain = gains_ref[layer : layer + 1, cols]
+                nrm[at, cols] = (f * inv * gain).astype(BF16)
+            return carry
+
+        lax.fori_loop(0, pieces, one, 0)
+
+    def project(idx):
+        total = None
+        for j in range(n_sp):
+            term = jnp.dot(
+                nrm[:, j * depth : (j + 1) * depth],
+                win[idx, j].reshape(depth, chans),
+                preferred_element_type=F32,
+            )
+            total = term if total is None else total + term
+        return total.astype(BF16).astype(F32)
+
+    def halo_copy(layer):
+        return pltpu.make_async_remote_copy(
+            src_ref=ext.at[layer, pl.ds(rows, 8)],
+            dst_ref=halo.at[layer],
+            send_sem=sem_h.at[layer, 0],
+            recv_sem=sem_h.at[layer, 1],
+            device_id=up(),
+            device_id_type=MESH,
+        )
+
+    def carry_copy(layer, d):
+        return pltpu.make_async_remote_copy(
+            src_ref=cry_out.at[layer],
+            dst_ref=cry_in.at[layer, s],
+            send_sem=sem_c_send.at[layer, d],
+            recv_sem=sem_c_recv.at[layer, s],
+            device_id={"sp": s + d},
+            device_id_type=MESH,
+        )
+
+    def carry_wait(layer, j):
+        pltpu.make_async_remote_copy(
+            src_ref=cry_out.at[layer],
+            dst_ref=cry_in.at[layer, j],
+            send_sem=sem_c_send.at[layer, 0],
+            recv_sem=sem_c_recv.at[layer, j],
+            device_id={"sp": s},
+            device_id_type=MESH,
+        ).wait_recv()
+
+    def rs_copy(src, dst, layer, k, where):
+        return pltpu.make_async_remote_copy(
+            src_ref=src,
+            dst_ref=dst,
+            send_sem=sem_rs_send.at[layer, k],
+            recv_sem=sem_rs_recv.at[layer, k],
+            device_id={"tp": where},
+            device_id_type=MESH,
+        )
+
+    def near_copy(layer, q):
+        to = lax.rem(sib + 2 * q, n_tp)
+        return rs_copy(part.at[layer, to], from_sib.at[layer, q], layer, q, sib)
+
+    def far_copy(layer, q):
+        where = lax.rem(t + 2 * q, n_tp)
+        return rs_copy(pair.at[layer, q], from_far.at[layer, q], layer, chips + q, where)
+
+    for layer in range(layers):
+        m0 = 3 * layer
+        src = x_ref if layer == 0 else xs.at[layer]
+        agx[layer, t] = src[...]
+        ag_finish(layer, src)
+        normalize(layer)
+        pump(m0)
+        arrived(m0)
+        ext[layer, 8:] = project(2 * layer)
+
+        @pl.when(s < n_sp - 1)
+        def _():
+            halo_copy(layer).start()
+
+        @pl.when(s == 0)
+        def _():
+            halo[layer] = jnp.zeros((8, chans), F32)
+
+        @pl.when(s > 0)
+        def _():
+            halo_copy(layer).wait_recv()
+
+        ext[layer, :8] = halo[layer]
+        n_taps = taps_ref.shape[1]
+        base = 8 - (n_taps - 1)
+        for b in range(chans // BLOCK_W):
+            cols = slice(b * BLOCK_W, (b + 1) * BLOCK_W)
+            conv = jnp.zeros((rows, BLOCK_W), F32)
+            for k in range(n_taps):
+                tap = taps_ref[layer, k : k + 1, cols].astype(F32)
+                conv = conv + ext[layer, base + k : base + k + rows, cols] * tap
+            conv = conv.astype(BF16)
+            reset = jax.nn.sigmoid(
+                jnp.dot(conv, reset_w[layer, b], preferred_element_type=F32)
+            )
+            inject = jax.nn.sigmoid(
+                jnp.dot(conv, inject_w[layer, b], preferred_element_type=F32)
+            )
+            log_keep = (
+                reset * rate_ref[layer : layer + 1, cols] * mult_ref[...]
+                + spike_ref[:, cols]
+            )
+            keep = jnp.exp(log_keep)
+            state = inject * conv.astype(F32) * jnp.sqrt(one_minus_exp(2.0 * log_keep))
+            lag = 1
+            while lag < rows:
+                state = keep * shifted(state, lag, 0.0) + state
+                keep = keep * shifted(keep, lag, 1.0)
+                lag *= 2
+            keep_s[:, cols] = keep
+            state_s[:, cols] = state
+            cry_out[layer, 0:1, cols] = keep[rows - 1 :]
+            cry_out[layer, 1:2, cols] = state[rows - 1 :]
+        for d in range(1, n_sp):
+
+            @pl.when(s + d < n_sp)
+            def _():
+                carry_copy(layer, d).start()
+
+        pump(m0 + 1)
+        arrived(m0 + 1)
+        gel_s[...] = jax.nn.gelu(project(2 * layer + 1))
+        hacc[...] = jnp.zeros((1, chans), F32)
+        for j in range(n_sp - 1):
+
+            @pl.when(j < s)
+            def _():
+                carry_wait(layer, j)
+                hacc[...] = cry_in[layer, j, 0:1] * hacc[...] + cry_in[layer, j, 1:2]
+
+        mix_s[...] = (
+            gel_s[...] * (state_s[...] + keep_s[...] * hacc[...])
+        ).astype(BF16)
+        pump(m0 + 2)
+        arrived(m0 + 2)
+        unit = min(depth, feats)
+        for j in range(n_sp):
+            done = jnp.dot(
+                mix_s[...],
+                wout[layer, j].reshape(chans, depth),
+                preferred_element_type=F32,
+            ).astype(BF16)
+            for c in range(0, depth, unit):
+                at = j * depth + c
+                low = at % feats
+                part[layer, at // feats, :, low : low + unit] = done[:, c : c + unit]
+        for q in list(range(1, chips)) + [0]:
+            near_copy(layer, q).start()
+        for q in range(1, chips):
+            near_copy(layer, q).wait_recv()
+            to = lax.rem(t + 2 * q, n_tp)
+            pair[layer, q] = (
+                part[layer, to].astype(F32) + from_sib[layer, q].astype(F32)
+            ).astype(BF16)
+            far_copy(layer, q).start()
+        near_copy(layer, 0).wait_recv()
+        mixed = part[layer, t].astype(F32) + from_sib[layer, 0].astype(F32)
+        for q in range(1, chips):
+            far_copy(layer, q).wait_recv()
+            mixed = mixed + from_far[layer, q].astype(F32)
+        fresh = (src[...].astype(F32) + mixed).astype(BF16)
+        xs[layer + 1] = fresh
+        if layer + 1 < layers:
+            ag_start(layer + 1, xs.at[layer + 1])
+
+    last = xs[layers].astype(F32)
+    square = jnp.sum(last * last, axis=1, keepdims=True)
+    sq_out[...] = jnp.broadcast_to(square, (rows, 128)).T[0:8]
+
+    def sq_copy(d):
+        return pltpu.make_async_remote_copy(
+            src_ref=sq_out,
+            dst_ref=sq_in.at[d],
+            send_sem=sem_q_send.at[d],
+            recv_sem=sem_q_recv.at[d],
+            device_id={"tp": lax.rem(t + d, n_tp)},
+            device_id_type=MESH,
+        )
+
+    for d in range(1, n_tp):
+        sq_copy(d).start()
+    total = sq_out[0:1]
+    for d in range(1, n_tp):
+        sq_copy(d).wait_recv()
+        total = total + sq_in[d, 0:1]
+    inv = lax.rsqrt(total / full + EPSILON)
+    inv = jnp.broadcast_to(inv, (128, rows)).T[:, 0:1]
+    out_ref[...] = (xs[layers].astype(F32) * inv * final_ref[...]).astype(BF16)
+
+    close_weights()
+    for layer in range(layers):
+        ag_close(layer, x_ref if layer == 0 else xs.at[layer])
+
+        @pl.when(s < n_sp - 1)
+        def _():
+            halo_copy(layer).wait_send()
+
+        for d in range(1, n_sp):
+
+            @pl.when(s + d < n_sp)
+            def _():
+                carry_copy(layer, d).wait_send()
+
+        for q in range(chips):
+            near_copy(layer, q).wait_send()
+        for q in range(1, chips):
+            far_copy(layer, q).wait_send()
+    for d in range(1, n_tp):
+        sq_copy(d).wait_send()
+
+
+def in_one_kernel(
+    sizes_of,
+    starting_stream,
+    multiplier_matrix,
+    memory_path_matrix,
+    filter_coefficients,
+    memory_valve_matrix,
+    entry_valve_matrix,
+    forgetting_parameters,
+    timestep_forgetting_multiplier,
+    spike_extra,
+    exit_projector_matrix,
+    prelude_rms_gains,
+    finishing_rms_gains,
+):
+    n_grp, n_sp, n_tp = sizes_of
+    rows, feats = starting_stream.shape
+    layers, depth, chans = memory_path_matrix.shape
+    pieces = rows // 128 if rows % 128 == 0 else 1
+    sizes = (layers, n_sp, n_tp, n_grp, rows, chans, feats, depth, pieces)
+    chips = n_tp // 2
+    half_in = (layers, 2, depth // 2, chans)
+    half_out = (layers, 2, chans // 2, depth)
+    rate = -SQUASH_POWER * jax.nn.softplus(-forgetting_parameters)
+    vmem = pl.BlockSpec(memory_space=pltpu.VMEM)
+    hbm = pl.BlockSpec(memory_space=pl.ANY)
+    count = 3 * layers
+    dma = pltpu.SemaphoreType.DMA
+    return pl.pallas_call(
+        functools.partial(fused, sizes),
+        out_shape=jax.ShapeDtypeStruct((rows, feats), BF16),
+        in_specs=[vmem, hbm, hbm, hbm] + [vmem] * 8,
+        out_specs=vmem,
+        scratch_shapes=[
+            pltpu.VMEM((2 * layers, n_sp, 2, depth // 2, chans), BF16),
+            pltpu.VMEM((layers, n_sp, 2, chans // 2, depth), BF16),
+            pltpu.VMEM((layers, n_tp, rows, feats), BF16),
+            pltpu.VMEM((layers + 1, rows, feats), BF16),
+            pltpu.VMEM((rows, n_tp * feats), BF16),
+            pltpu.VMEM((layers, 8 + rows, chans), F32),
+            pltpu.VMEM((layers, 8, chans), F32),
+            pltpu.VMEM((rows, chans), F32),
+            pltpu.VMEM((rows, chans), F32),
+            pltpu.VMEM((rows, chans), F32),
+            pltpu.VMEM((rows, chans), BF16),
+            pltpu.VMEM((layers, n_tp, rows, feats), BF16),
+            pltpu.VMEM((layers, chips, rows, feats), BF16),
+            pltpu.VMEM((layers, chips, rows, feats), BF16),
+            pltpu.VMEM((layers, chips, rows, feats), BF16),
+            pltpu.VMEM((layers, 2, chans), F32),
+            pltpu.VMEM((layers, n_sp, 2, chans), F32),
+            pltpu.VMEM((1, chans), F32),
+            pltpu.VMEM((8, rows), F32),
+            pltpu.VMEM((n_tp, 8, rows), F32),
+            dma((count,)),
+            dma((count, n_sp, 2)),
+            dma((count, n_sp)),
+            dma((count, n_sp)),
+            dma((count, n_sp)),
+            dma((layers, 2 * chips)),
+            dma((layers, n_tp)),
+            dma((layers, 2 * chips)),
+            dma((layers, 2 * chips)),
+            dma((layers, 2)),
+            dma((layers, n_sp)),
+            dma((layers, n_sp)),
+            dma((n_tp,)),
+            dma((n_tp,)),
+        ],
+        compiler_params=pltpu.CompilerParams(
+            collective_id=0, has_side_effects=True, vmem_limit_bytes=60 * 2**20
+        ),
+    )(
+        starting_stream,
+        multiplier_matrix.reshape(half_in),
+        memory_path_matrix.reshape(half_in),
+        exit_projector_matrix.reshape(half_out),
+        filter_coefficients,
+        memory_valve_matrix,
+        entry_valve_matrix,
+        rate,
+        timestep_forgetting_multiplier.reshape(rows, 1),
+        spike_extra,
+        prelude_rms_gains,
+        finishing_rms_gains.reshape(1, feats),
+    )
+
+
+def on_each(sizes_of, *arrays):
+    stream, memory = arrays[0], arrays[2]
+    n_grp, n_sp, n_tp = sizes_of
+    rows, feats = stream.shape
+    depth, chans = memory.shape[1:]
+    unit = min(depth, feats)
+    fits = (
+        n_grp == 2
+        and n_sp > 1
+        and n_tp % 2 == 0
+        and rows % 128 == 0
+        and depth % 128 == 0
+        and feats % 128 == 0
+        and chans % BLOCK_W == 0
+        and depth % unit == 0
+        and feats % unit == 0
+    )
+    if fits:
+        return in_one_kernel(sizes_of, *arrays)
+    return on_device(*arrays)
+
+
 def solution(mesh):
+    sizes_of = tuple(mesh.shape[axis] for axis in ("grp", "sp", "tp"))
+    body = functools.partial(on_each, sizes_of)
     return jax.shard_map(
-        on_device,
+        body,
         mesh=mesh,
         in_specs=(
             P(("grp", "sp"), "tp"),

time: 501 us -> 195 us (0.39)
  waiting for transfers between devices: 216 us -> 0 us
  Pallas kernels: 0 us -> 191 us
  local copies, waits for them, and re-layouts: 118 us -> 3.31 us
  other arithmetic: 65.8 us -> 0.61 us
  blocking collectives: 56.4 us -> 0 us
  matrix products: 20.7 us -> 0 us
  between operations: 14.9 us -> 0.01 us
    pallas_call x0 -> x1, Pallas kernels: none -> 191 us  [in_one_kernel(): pl.pallas_call(functools.partial(fused, sizes), out_shape=jax.ShapeDtypeS...]
    all_gather x8 -> x0, waiting for transfers between devices: 158 us -> none  [the longest x2 90.9 us: on_device(): lax.all_gather(memory_path_matrix[tier_number], 'sp', axis=0, tiled=True)]
    slice x118 -> x0, local copies, waits for them, and re-layouts: 66.7 us -> none  [the longest x112 61.7 us: on_device(): lax.associative_scan(combine_pairs, (keep_rate, driven), axis=0)]
    reduce_scatter x2 -> x0, waiting for transfers between devices: 53.7 us -> none  [on_device(): lax.psum_scatter(partial_value.astype(jnp.bfloat16), 'tp', scatter_dimens...]
    all_gather x4 -> x0, blocking collectives: 50.6 us -> none  [entering(): gathered = jax.tree.map(lambda a: lax.all_gather(a, axis), part)]
    pad x60 -> x0, local copies, waits for them, and re-layouts: 46.7 us -> none  [on_device(): lax.associative_scan(combine_pairs, (keep_rate, driven), axis=0)]
    add x57 -> x0, other arithmetic: 35.7 us -> none  [the longest x30 19.8 us: combine_pairs(): return (earlier[0] * later[0], later[0] * earlier[1] + later[1])]
    dot_general x8 -> x0, matrix products: 20.7 us -> none  [the longest x2 12.7 us: on_device(): jnp.dot(mixed_in, lax.all_gather(exit_projector_matrix[tier_number], 'sp'...]
  transfers between devices with their start and end apart: 12 -> 0, of which waited for: 9 -> 0; matrix products, arithmetic and copies ran while one was open for 37% -> 0% of each run, Pallas kernels for 0% -> 0%
where the time goes in v1:
time: 195 us
  Pallas kernels  191 us (98%)
  local copies, waits for them, and re-layouts  3.31 us (2%)
    pallas_call x1, Pallas kernels, in_one_kernel(): pl.pallas_call(functools.partial(fused, sizes), out_shape=jax.ShapeDtypeS...  191 us

profile of v1, /device:TPU:0, one launch (start us, length us, event | category | flops | bytes accessed | tf_op | source)
XLA Modules:
  0.0 194.8 jit_solution(537306259993099160)
XLA Ops:
  0.0 0.0 copy-start
  0.0 0.7 copy-done
  0.7 0.0 copy-start.1
  0.7 0.6 fusion.rate_ref
  1.3 0.1 copy-done.1
  1.4 0.8 reshape.20.mult_ref
  2.2 190.9 %shard_map.118 = bf16[384,512]{1,0:T(8,128)(2,1)} custom-call(bf16[384,512]{1,0:T(8,128)(2,1)} %x_ref.1, bf16[2,2,256,512]{3,2,1,0:T(8,128)(2,1)} %bitcast.4, bf16[2,2,256,512]{3,2,1,0:T(8,128)(2,1)} %bitcast.5, bf16[2,2,256,512]{3,2,1,0:T(8,128)(2,1)} %bitcast.6, bf16[2,4,512]{2,1,0:T(4,128)(2,1)} %taps_ref.1, bf16[2,2,256,256]{3,2,1,0:T(8,128)(2,1)} %reset_w.1, ...), custom_call_target="tpu_custom_call" | custom-call | tf_op jit(solution)/shard_map/pallas_call | solution.py:622
  193.1 1.8 copy.15
Async XLA Ops:
  0.0 0.7 copy-start
  0.7 0.7 copy-start.1

commit v2 on v1

--- a/solution.py
+++ b/solution.py
@@ -269,42 +269,54 @@
     def keep_own(m):
         return pltpu.make_async_copy(own_block(m), held(m, s), sem_own.at[m])
 
-    def pump(m):
-        for d in range(1, n_sp):
-
-            @pl.when(s - d >= 0)
-            def _():
-                j = s - d
-                src = held(m, j).at[g]
-                sent(src, m, j, g, sem_up, up()).wait_recv()
-
-                @pl.when(s < n_sp - 1)
-                def _():
-                    sent(src, m, j, g, sem_up, up()).start()
-
-                sent(src, m, j, g, sem_y, across()).start()
-
-            @pl.when(s + d < n_sp)
-            def _():
-                j = s + d
-                src = held(m, j).at[g]
-                sent(src, m, j, g, sem_down, down()).wait_recv()
-
-                @pl.when(s > 0)
-                def _():
-                    sent(src, m, j, g, sem_down, down()).start()
-
-                sent(src, m, j, g, sem_y, across()).start()
-
-        if m + 3 < 3 * layers:
-            start_own(m + 3)
+    items = [(m, d) for m in range(3 * layers) for d in range(1, n_sp)]
+    place = [0]
+
+    def pump(m, d):
+        @pl.when(s - d >= 0)
+        def _():
+            j = s - d
+            src = held(m, j).at[g]
+            sent(src, m, j, g, sem_up, up()).wait_recv()
+
+            @pl.when(s < n_sp - 1)
+            def _():
+                sent(src, m, j, g, sem_up, up()).start()
+
+            sent(src, m, j, g, sem_y, across()).start()
+
+        @pl.when(s + d < n_sp)
+        def _():
+            j = s + d
+            src = held(m, j).at[g]
+            sent(src, m, j, g, sem_down, down()).wait_recv()
+
+            @pl.when(s > 0)
+            def _():
+                sent(src, m, j, g, sem_down, down()).start()
+
+            sent(src, m, j, g, sem_y, across()).start()
+
+        if d == n_sp - 1 and m + 2 < 3 * layers:
+            start_own(m + 2)
+
+    def advance(steps):
+        for m, d in items[place[0] : place[0] + steps]:
+            pump(m, d)
+        place[0] = min(place[0] + steps, len(items))
+
+    def reach(m, d):
+        advance(max(0, m * (n_sp - 1) + d - place[0]))
+
+    def swapped(m, j):
+        src = held(m, j).at[1 - g]
+        sent(src, m, j, 1 - g, sem_y, across()).wait_recv()
 
     def arrived(m):
+        reach(m, n_sp - 1)
         keep_own(m).wait()
         for d in range(1, n_sp):
-            j = lax.rem(s + d, n_sp)
-            src = held(m, j).at[1 - g]
-            sent(src, m, j, 1 - g, sem_y, across()).wait_recv()
+            swapped(m, lax.rem(s + d, n_sp))
 
     def close_weights():
         for m in range(3 * layers):
@@ -359,7 +371,7 @@
         ag_copy(src, layer, t, 0, sib).wait_send()
 
     ag_start(0, x_ref)
-    for m in range(min(3, 3 * layers)):
+    for m in range(2):
         start_own(m)
 
     step = rows // pieces
@@ -444,15 +456,19 @@
         m0 = 3 * layer
         src = x_ref if layer == 0 else xs.at[layer]
         agx[layer, t] = src[...]
+        advance(1)
         ag_finish(layer, src)
+        advance(1)
         normalize(layer)
-        pump(m0)
+        reach(m0, n_sp)
         arrived(m0)
         ext[layer, 8:] = project(2 * layer)
 
         @pl.when(s < n_sp - 1)
         def _():
             halo_copy(layer).start()
+
+        advance(1)
 
         @pl.when(s == 0)
         def _():
@@ -493,13 +509,14 @@
             state_s[:, cols] = state
             cry_out[layer, 0:1, cols] = keep[rows - 1 :]
             cry_out[layer, 1:2, cols] = state[rows - 1 :]
+            advance(1)
         for d in range(1, n_sp):
 
             @pl.when(s + d < n_sp)
             def _():
                 carry_copy(layer, d).start()
 
-        pump(m0 + 1)
+        reach(m0 + 2, min(2, n_sp - 1))
         arrived(m0 + 1)
         gel_s[...] = jax.nn.gelu(project(2 * layer + 1))
         hacc[...] = jnp.zeros((1, chans), F32)
@@ -513,28 +530,65 @@
         mix_s[...] = (
             gel_s[...] * (state_s[...] + keep_s[...] * hacc[...])
         ).astype(BF16)
-        pump(m0 + 2)
-        arrived(m0 + 2)
-        unit = min(depth, feats)
-        for j in range(n_sp):
-            done = jnp.dot(
+        def chips_on(j):
+            return lax.rem(j // 2 - chip + chips, chips)
+
+        def product(j):
+            part[layer, j] = jnp.dot(
                 mix_s[...],
                 wout[layer, j].reshape(chans, depth),
                 preferred_element_type=F32,
             ).astype(BF16)
-            for c in range(0, depth, unit):
-                at = j * depth + c
-                low = at % feats
-                part[layer, at // feats, :, low : low + unit] = done[:, c : c + unit]
-        for q in list(range(1, chips)) + [0]:
-            near_copy(layer, q).start()
-        for q in range(1, chips):
-            near_copy(layer, q).wait_recv()
-            to = lax.rem(t + 2 * q, n_tp)
-            pair[layer, q] = (
-                part[layer, to].astype(F32) + from_sib[layer, q].astype(F32)
-            ).astype(BF16)
-            far_copy(layer, q).start()
+
+            @pl.when(lax.rem(j, 2) != core)
+            def _():
+                near_copy(layer, chips_on(j)).start()
+
+        def pass_on(j):
+            q = chips_on(j)
+
+            @pl.when((lax.rem(j, 2) == core) & (q != 0))
+            def _():
+                near_copy(layer, q).wait_recv()
+                pair[layer, q] = (
+                    part[layer, j].astype(F32) + from_sib[layer, q].astype(F32)
+                ).astype(BF16)
+                far_copy(layer, q).start()
+
+        m = m0 + 2
+        keep_own(m).wait()
+        product(s)
+        for d in range(1, n_sp):
+            reach(m, d)
+            if d > 1:
+                advance(1)
+
+            @pl.when(s - d >= 0)
+            def _():
+                swapped(m, s - d)
+                product(s - d)
+
+            @pl.when(s + d < n_sp)
+            def _():
+                swapped(m, s + d)
+                product(s + d)
+
+            if d == 1:
+                pass_on(s)
+            else:
+                for j in (s - d + 1, s + d - 1):
+
+                    @pl.when((j >= 0) & (j < n_sp))
+                    def _():
+                        pass_on(j)
+
+        for j in (s - n_sp + 1, s + n_sp - 1):
+
+            @pl.when((j >= 0) & (j < n_sp))
+            def _():
+                pass_on(j)
+
+        advance(1)
         near_copy(layer, 0).wait_recv()
         mixed = part[layer, t].astype(F32) + from_sib[layer, 0].astype(F32)
         for q in range(1, chips):
@@ -684,7 +738,6 @@
     n_grp, n_sp, n_tp = sizes_of
     rows, feats = stream.shape
     depth, chans = memory.shape[1:]
-    unit = min(depth, feats)
     fits = (
         n_grp == 2
         and n_sp > 1
@@ -693,8 +746,8 @@
         and depth % 128 == 0
         and feats % 128 == 0
         and chans % BLOCK_W == 0
-        and depth % unit == 0
-        and feats % unit == 0
+        and depth == feats
+        and n_sp == n_tp
     )
     if fits:
         return in_one_kernel(sizes_of, *arrays)

time: 195 us -> 153 us (0.78)
  Pallas kernels: 191 us -> 149 us
    pallas_call x1, Pallas kernels: 191 us -> 149 us  [in_one_kernel(): pl.pallas_call(functools.partial(fused, sizes), out_shape=jax.ShapeDtypeS...]
where the time goes in v2:
time: 153 us
  Pallas kernels  149 us (97%)
  local copies, waits for them, and re-layouts  3.31 us (2%)
    pallas_call x1, Pallas kernels, in_one_kernel(): pl.pallas_call(functools.partial(fused, sizes), out_shape=jax.ShapeDtypeS...  149 us

profile of v2, /device:TPU:0, one launch (start us, length us, event | category | flops | bytes accessed | tf_op | source)
XLA Modules:
  0.0 152.9 jit_solution(16187340898772377512)
XLA Ops:
  0.0 0.0 copy-start
  0.0 0.7 copy-done
  0.7 0.0 copy-start.1
  0.7 0.6 fusion.rate_ref
  1.3 0.1 copy-done.1
  1.4 0.8 reshape.20.mult_ref
  2.2 148.9 %shard_map.118 = bf16[384,512]{1,0:T(8,128)(2,1)} custom-call(bf16[384,512]{1,0:T(8,128)(2,1)} %x_ref.1, bf16[2,2,256,512]{3,2,1,0:T(8,128)(2,1)} %bitcast.4, bf16[2,2,256,512]{3,2,1,0:T(8,128)(2,1)} %bitcast.5, bf16[2,2,256,512]{3,2,1,0:T(8,128)(2,1)} %bitcast.6, bf16[2,4,512]{2,1,0:T(4,128)(2,1)} %taps_ref.1, bf16[2,2,256,256]{3,2,1,0:T(8,128)(2,1)} %reset_w.1, ...), custom_call_target="tpu_custom_call" | custom-call | tf_op jit(solution)/shard_map/pallas_call | solution.py:676
  151.1 1.8 %copy.15 = bf16[384,512]{1,0:T(8,128)(2,1)} copy(bf16[384,512]{1,0:T(8,128)(2,1)} %shard_map.118) | data formatting | bytes 786432
Async XLA Ops:
  0.0 0.7 copy-start
  0.7 0.7 copy-start.1
